TPU v7x, 32 devices: a whole 2x2x4 slice. The times are simulated.
32 devices in a mesh: fs: 8 (over z, y), tp: 4 (over x, core).
Axes of the slice: x: 2, y: 2, z: 4, core: 2. Of those that a mesh axis runs over, the one named last changes fastest.
Arguments:
- prompt: bfloat16 [4096, 4096], P('fs'), may hold values from -6 to 6
- expert_ids: int32 [4096, 2], P('fs'), may hold values from 0 to 15, all different within a row; in each aligned block of 512 rows (0 to 511, 512 to 1023, ...) at most 96 rows name the same one
- group_weight: float32 [4096], P('fs'), may hold values from 0.25 to 1
- expert_share: float32 [4096, 2], P('fs'), may hold values from 0.1 to 1
- norm_gain: float32 [4096], P('fs'), may hold values from 0.1 to 1.9
- gate_train: float32 [16, 4096, 1024], P(None, 'fs', 'tp'), may hold values from -0.09375 to 0.09375
- up_train: float32 [16, 4096, 1024], P(None, 'fs', 'tp'), may hold values from -0.09375 to 0.09375
- down_train: float32 [16, 1024, 4096], P(None, 'fs', 'tp'), may hold values from -0.1875 to 0.1875
Outputs:
- mixed: bfloat16 [4096, 4096], P('fs', 'tp')
- gate_new: bfloat16 [16, 4096, 1024], P('fs', None, 'tp')
- up_new: bfloat16 [16, 4096, 1024], P('fs', None, 'tp')
- down_new: bfloat16 [16, 1024, 4096], P('fs', 'tp')
Inputs may be any that keep to these rules, and one draw needn't show every extreme that they name: `expert_ids`: each row names two different experts; within the rows of one index of fs no expert is named more than 96 times, a bound that some block reaches there.
All inputs are finite; a program needn't handle non-finite values.
Results may differ from a plain program's by a relative error of at most 0.0086.
Values may be sent and summed in bfloat16 or wider, within the bound.
A program may use at most 128 MiB of HBM per device.

v0:
```python
import functools

import jax
import jax.numpy as jnp
from jax import lax
from jax.experimental import pallas as pl
from jax.experimental.pallas import tpu as pltpu
from jax.sharding import PartitionSpec as P

EPS = 1e-06
MESH = pl.DeviceIdType.MESH
BF16 = jnp.bfloat16
F32 = jnp.float32
PROMPT_STEPS = 4


def kernel(
    n,
    tp,
    prompt,
    ids,
    group,
    share,
    gain,
    gate_hbm,
    up_hbm,
    down_hbm,
    mixed_out,
    gate_out,
    up_out,
    down_out,
    wide,
    tall,
    gate_send,
    up_send,
    gate_land,
    up_land,
    down_land,
    rows_stage,
    piece,
    own_cols,
    far_cols,
    facts,
    far_facts,
    gain_cols,
    hid,
    gate_acc,
    spread,
    ret_stage,
    ret_land,
    far_stage,
    far_land,
    total,
    mixed_tile,
    load_sem,
    tall_sem,
    out_sem,
    send_sem,
    recv_sem,
    down_recv,
    chip_recv,
    mate_recv,
    hid_chip_recv,
    hid_mate_recv,
    ret_recv,
    far_recv,
):
    here = lax.axis_index("fs")
    me = lax.axis_index("tp")
    half = n // 2
    side = here // half
    seat = here % half
    partner = (here + half) % n
    mate = me + 1 - 2 * (me % 2)
    chips = tp // 2
    tokens, model_width = prompt.shape
    experts_all, depth, units = gate_hbm.shape
    local = experts_all // n
    capacity = ret_land.shape[4]
    own_width = own_cols.shape[1]
    down_depth = down_hbm.shape[1]
    chunks, width = down_land.shape[0], down_land.shape[3]
    seat_slots = local * capacity
    GATE, UP, DOWN, FACTS, COLS, ROWS, PIECE, HID, RET, FAR, TALL = range(11)

    def remote(src, dst, ssem, rsem, fs=None, tp_to=None):
        device = {"fs": here if fs is None else fs, "tp": me if tp_to is None else tp_to}
        return pltpu.make_async_remote_copy(
            src_ref=src,
            dst_ref=dst,
            send_sem=ssem,
            recv_sem=rsem,
            device_id=device,
            device_id_type=MESH,
        )

    def drain(ref, sem):
        pltpu.make_async_copy(ref, ref, sem).wait()

    def shift_of(k):
        return half + (k + 1) // 2 * (1 - 2 * (k % 2))

    def owner_of(k):
        return lax.rem(here + jnp.where(k == n - 1, 0, shift_of(k)), n)

    barrier = pltpu.get_barrier_semaphore()

    @pl.loop(1, n)
    def _(s):
        pl.semaphore_signal(
            barrier, inc=1, device_id={"fs": lax.rem(here + s, n), "tp": me}, device_id_type=MESH
        )

    @pl.loop(1, tp)
    def _(s):
        pl.semaphore_signal(
            barrier, inc=1, device_id={"fs": here, "tp": lax.rem(me + s, tp)}, device_id_type=MESH
        )

    def load(source, k):
        return pltpu.make_async_copy(
            source.at[pl.ds(owner_of(k) * local, local)], wide.at[k % 2], load_sem.at[k % 2]
        )

    def load_down(k, c):
        return pltpu.make_async_copy(
            down_hbm.at[pl.ds(owner_of(k) * local, local), :, pl.ds(c * width, width)],
            wide.at[k % 2, :, pl.ds(c * down_depth, down_depth), :],
            load_sem.at[k % 2],
        )

    block_rows = tokens // PROMPT_STEPS

    def load_prompt(i):
        return pltpu.make_async_copy(
            prompt.at[pl.ds(i * block_rows, block_rows)], tall.at[i % 2], tall_sem.at[i % 2]
        )

    load(gate_hbm, 0).start()
    load(gate_hbm, 1).start()
    load_prompt(0).start()
    load_prompt(1).start()

    lanes = min(128, depth)
    gain_cols[...] = jnp.transpose(jnp.broadcast_to(gain[...], (128, depth)))

    def cast(slot, out):
        for e in range(local):
            for j in range(units // 128):
                cols = pl.ds(j * 128, 128)
                out[e, :, cols] = (wide[slot, e, :, cols] * gain_cols[...]).astype(BF16)

    def send_weight(send, land, which, k):
        return remote(
            send.at[k],
            land.at[:, pl.ds(here * depth, depth), :],
            send_sem.at[which],
            recv_sem.at[which],
            fs=owner_of(k),
        )

    def weight_steps(source, send, land, which, first, last):
        @pl.loop(first, last)
        def _(k):
            load(source, k).wait()
            cast(k % 2, send.at[k])

            @pl.when(k + 2 < n)
            def _():
                load(source, k + 2).start()

            @pl.when(k > first)
            def _():
                send_weight(send, land, which, k - 1).start()

        send_weight(send, land, which, last - 1).start()

    def own_weight(source, land):
        load(source, n - 1).wait()
        cast((n - 1) % 2, land.at[:, pl.ds(here * depth, depth), :])

    for k in range(2):
        load(gate_hbm, k).wait()
        cast(k % 2, gate_send.at[k])
        load(gate_hbm, k + 2).start()
    pl.semaphore_wait(barrier, n - 1 + tp - 1)
    for k in range(2):
        send_weight(gate_send, gate_land, GATE, k).start()

    experts = lax.broadcasted_iota(jnp.int32, (experts_all, tokens), 0)
    named = [experts == ids[pl.ds(k, 1), :] for k in range(2)]
    count = sum(m.astype(F32) for m in named).astype(BF16)
    earlier = (
        lax.broadcasted_iota(jnp.int32, (tokens, tokens), 0)
        < lax.broadcasted_iota(jnp.int32, (tokens, tokens), 1)
    ).astype(F32).astype(BF16)
    ranks = jnp.dot(count, earlier, preferred_element_type=F32)
    shares = [share[pl.ds(k, 1), :] for k in range(2)]
    facts[...] = jnp.zeros_like(facts)
    for k in range(2):
        rank = jnp.sum(jnp.where(named[k], ranks, 0.0), axis=0, keepdims=True)
        facts[pl.ds(k, 1), :] = ids[pl.ds(k, 1), :].astype(F32) * capacity + rank
        facts[pl.ds(2 + k, 1), :] = group[...] * shares[k] / (shares[0] + shares[1])

    @pl.loop(0, PROMPT_STEPS)
    def _(i):
        load_prompt(i).wait()
        squares = jnp.zeros((block_rows, 128), F32)
        for j in range(model_width // 128):
            x = tall[i % 2, :, pl.ds(j * 128, 128)].astype(F32)
            squares += x * x
        mean = jnp.sum(squares, axis=1, keepdims=True) / model_width
        scale = lax.rsqrt(mean + EPS)
        cols = pl.ds(pl.multiple_of(me * own_width, 128), own_width)
        own_cols[pl.ds(pl.multiple_of(i * block_rows, block_rows), block_rows), :] = (
            tall[i % 2, :, cols].astype(F32) * scale
        ).astype(BF16)

        @pl.when(i + 2 < PROMPT_STEPS)
        def _():
            load_prompt(i + 2).start()

    send_facts = remote(
        facts, far_facts, send_sem.at[FACTS], recv_sem.at[FACTS], fs=partner
    )
    send_cols = remote(own_cols, far_cols, send_sem.at[COLS], recv_sem.at[COLS], fs=partner)
    send_facts.start()
    send_cols.start()

    weight_steps(gate_hbm, gate_send, gate_land, GATE, 2, n - 1)
    own_weight(gate_hbm, gate_land)
    load(up_hbm, 0).start()
    load(up_hbm, 1).start()

    def send_rows(q, j):
        to = lax.rem(seat + j, half)
        return remote(
            rows_stage.at[q, to],
            piece.at[me, :, pl.ds(pl.multiple_of((seat * 2 + q) * capacity, 16), capacity), :],
            send_sem.at[ROWS],
            recv_sem.at[ROWS],
            fs=side * half + to,
        )

    def place_rows(q, block_facts, columns):
        targets = [block_facts[pl.ds(k, 1), :].astype(jnp.int32) for k in range(2)]

        @pl.loop(0, half)
        def _(j):
            to = lax.rem(seat + j, half)
            slots = (side * half + to) * seat_slots + lax.broadcasted_iota(
                jnp.int32, (seat_slots, tokens), 0
            )
            picker = ((slots == targets[0]) | (slots == targets[1])).astype(F32).astype(BF16)
            rows = jnp.dot(picker, columns[...], preferred_element_type=F32)
            rows_stage[q, to] = rows.astype(BF16).reshape(local, capacity, own_width)

            @pl.when(j == 0)
            def _():
                piece[
                    me, :, pl.ds(pl.multiple_of((seat * 2 + q) * capacity, 16), capacity), :
                ] = rows_stage[q, seat]

            @pl.when(j > 1)
            def _():
                send_rows(q, j - 1).start()

        send_rows(q, half - 1).start()

    place_rows(0, facts, own_cols)
    send_facts.wait_recv()
    send_cols.wait_recv()
    place_rows(1, far_facts, far_cols)

    weight_steps(up_hbm, up_send, up_land, UP, 0, n - 1)
    own_weight(up_hbm, up_land)

    drain(gate_send, send_sem.at[GATE])

    @pl.loop(0, 2)
    def _(k):
        for c in range(chunks):
            load_down(k, c).start()

    def cast_down(k, out):
        for c in range(chunks):
            load_down(k, c).wait()
        for e in range(local):
            out[e] = wide[k % 2, e].astype(BF16)

        @pl.when(k + 2 < n)
        def _():
            for c in range(chunks):
                load_down(k + 2, c).start()

    @pl.loop(0, n - 1)
    def _(k):
        cast_down(k, gate_send.at[k])

    for c in range(chunks):
        load_down(n - 1, c).wait()
    for c in range(chunks):
        for e in range(local):
            down_land[c, e, pl.ds(pl.multiple_of(here * down_depth, 16), down_depth), :] = wide[
                (n - 1) % 2, e, pl.ds(c * down_depth, down_depth), :
            ].astype(BF16)

    @pl.loop(0, chunks)
    def _(c):
        @pl.loop(0, n - 1)
        def _(k):
            remote(
                gate_send.at[k, :, pl.ds(pl.multiple_of(c * down_depth, 16), down_depth), :],
                down_land.at[
                    c, :, pl.ds(pl.multiple_of(here * down_depth, 16), down_depth), :
                ],
                send_sem.at[DOWN],
                down_recv.at[c],
                fs=owner_of(k),
            ).start()

    def chip_peer(j):
        return lax.rem(me + 2 * j, tp)

    def chip_from(j):
        return lax.rem(me + tp - 2 * j, tp)

    def spread_tp(buffer, which, chip_sems, mate_sems):
        mine = buffer.at[me]

        @pl.loop(1, chips)
        def _(j):
            remote(mine, mine, send_sem.at[which], chip_sems.at[j - 1], tp_to=chip_peer(j)).start()

        remote(mine, mine, send_sem.at[which], mate_sems.at[0], tp_to=mate).start()

    def forward_tp(buffer, which, chip_sems, mate_sems):
        @pl.loop(1, chips)
        def _(j):
            theirs = buffer.at[chip_from(j)]
            pltpu.make_async_copy(theirs, theirs, chip_sems.at[j - 1]).wait()
            remote(theirs, theirs, send_sem.at[which], mate_sems.at[j], tp_to=mate).start()

    def collect_tp(buffer, mate_sems):
        @pl.loop(0, chips)
        def _(j):
            theirs = buffer.at[0]
            pltpu.make_async_copy(theirs, theirs, mate_sems.at[j]).wait()

    drain(
        piece.at[me, :, pl.ds(0, (half - 1) * 2 * capacity), :], recv_sem.at[ROWS]
    )
    spread_tp(piece, PIECE, chip_recv, mate_recv)

    @pl.loop(0, half)
    def _(j):
        for q in range(2):
            source = (facts, far_facts)[q]
            slots = (side * half + j) * seat_slots + lax.broadcasted_iota(
                jnp.int32, (seat_slots, tokens), 0
            )
            value = sum(
                jnp.where(
                    slots == source[pl.ds(k, 1), :].astype(jnp.int32),
                    source[pl.ds(2 + k, 1), :],
                    0.0,
                )
                for k in range(2)
            )
            high = value.astype(BF16)
            at = pl.ds(pl.multiple_of(j * seat_slots, 16), seat_slots)
            spread[q, 0, at, :] = high
            spread[q, 1, at, :] = (value - high.astype(F32)).astype(BF16)

    forward_tp(piece, PIECE, chip_recv, mate_recv)

    drain(gate_land.at[:, pl.ds(0, (n - 1) * depth), :], recv_sem.at[GATE])
    store_gate = pltpu.make_async_copy(gate_land, gate_out, out_sem.at[0])
    store_gate.start()
    collect_tp(piece, mate_recv)

    def contracted(land, e):
        acc = None
        for t in range(tp):
            part = jnp.dot(
                piece[t, e],
                land[e, pl.ds(t * own_width, own_width), :],
                preferred_element_type=F32,
            )
            acc = part if acc is None else acc + part
        return acc

    @pl.loop(0, local)
    def _(e):
        gate_acc[e] = contracted(gate_land, e)

    drain(up_land.at[:, pl.ds(0, (n - 1) * depth), :], recv_sem.at[UP])
    store_up = pltpu.make_async_copy(up_land, up_out, out_sem.at[1])
    store_up.start()

    @pl.loop(0, local)
    def _(e):
        g = gate_acc[e]
        hid[me, e] = (g / (1.0 + jnp.exp(-g)) * contracted(up_land, e)).astype(BF16)

    spread_tp(hid, HID, hid_chip_recv, hid_mate_recv)
    forward_tp(hid, HID, hid_chip_recv, hid_mate_recv)
    collect_tp(hid, hid_mate_recv)

    def down_cols(c, t):
        return down_out.at[
            :, :, pl.ds(pl.multiple_of(t * own_width + c * width, 128), width)
        ]

    def send_tall(c, j):
        to = lax.rem(me + j, tp)
        return remote(
            down_land.at[c, :, pl.ds(pl.multiple_of(to * units, 16), units), :],
            down_cols(c, me),
            send_sem.at[TALL],
            recv_sem.at[TALL],
            tp_to=to,
        )

    def own_tall(c):
        return pltpu.make_async_copy(
            down_land.at[c, :, pl.ds(pl.multiple_of(me * units, 16), units), :],
            down_cols(c, me),
            out_sem.at[2],
        )

    def send_back(c, q, j):
        to = lax.rem(seat + j, half)
        return remote(
            ret_stage.at[c, :, pl.ds(pl.multiple_of((to * 2 + q) * capacity, 16), capacity), :],
            ret_land.at[c, q, seat],
            send_sem.at[RET],
            ret_recv.at[c],
            fs=side * half + to,
        )

    def combine(c):
        drain(ret_land.at[c, :, pl.ds(0, half - 1)], ret_recv.at[c])
        for q in range(2):
            back = ret_land[c, q].reshape(half * seat_slots, width)
            value = sum(
                lax.dot_general(
                    spread[q, p], back, (((0,), (0,)), ((), ())), preferred_element_type=F32
                )
                for p in range(2)
            )
            if q:
                far_stage[c] = value.astype(BF16)
            else:
                total[c] = value

    def send_far(c):
        return remote(
            far_stage.at[c], far_land.at[c], send_sem.at[FAR], far_recv.at[c], fs=partner
        )

    @pl.loop(0, chunks)
    def _(c):
        drain(down_land.at[c, :, pl.ds(0, (n - 1) * down_depth), :], down_recv.at[c])

        @pl.loop(0, local)
        def _(e):
            acc = None
            for t in range(tp):
                part = jnp.dot(
                    hid[t, e],
                    down_land[c, e, pl.ds(t * units, units), :],
                    preferred_element_type=F32,
                )
                acc = part if acc is None else acc + part
            ret_stage[c, e] = acc.astype(BF16)

        own_tall(c).start()

        @pl.loop(1, tp)
        def _(j):
            send_tall(c, j).start()

        @pl.loop(1, half)
        def _(j):
            for q in range(2):
                send_back(c, q, j).start()

        for q in range(2):
            ret_land[c, q, seat] = ret_stage[
                c, :, pl.ds(pl.multiple_of((seat * 2 + q) * capacity, 16), capacity), :
            ]

        @pl.when(c > 0)
        def _():
            combine(c - 1)

        @pl.when(c > 0)
        def _():
            send_far(c - 1).start()

    combine(chunks - 1)

    def store_mixed(c):
        return pltpu.make_async_copy(
            mixed_tile.at[c],
            mixed_out.at[:, pl.ds(pl.multiple_of(c * width, 128), width)],
            out_sem.at[3],
        )

    @pl.loop(0, chunks)
    def _(c):
        @pl.when(c == 0)
        def _():
            send_far(chunks - 1).start()

        pltpu.make_async_copy(far_land.at[c], far_land.at[c], far_recv.at[c]).wait()
        mixed_tile[c] = (total[c] + far_land[c].astype(F32)).astype(BF16)
        store_mixed(c).start()

    drain(up_send, send_sem.at[UP])
    drain(gate_send, send_sem.at[DOWN])
    send_facts.wait_send()
    send_cols.wait_send()
    drain(piece.at[0, :, pl.ds(0, (half - 1) * 2 * capacity), :], send_sem.at[ROWS])
    drain(piece.at[pl.ds(0, 2 * chips - 1)], send_sem.at[PIECE])
    drain(hid.at[pl.ds(0, 2 * chips - 1)], send_sem.at[HID])
    drain(ret_land.at[:, :, pl.ds(0, half - 1)], send_sem.at[RET])
    drain(far_land, send_sem.at[FAR])
    others = down_out.at[:, :, pl.ds(0, (tp - 1) * own_width)]
    drain(others, send_sem.at[TALL])
    drain(others, recv_sem.at[TALL])
    drain(down_out.at[:, :, pl.ds(0, own_width)], out_sem.at[2])
    drain(mixed_tile, out_sem.at[3])
    store_gate.wait()
    store_up.wait()


def on_device(
    prompt, expert_ids, group_weight, expert_share, norm_gain, gate_train, up_train, down_train
):
    n = lax.axis_size("fs")
    tp = lax.axis_size("tp")
    half = n // 2
    tokens, model_width = prompt.shape
    experts_all, depth, units = gate_train.shape
    down_depth, own_width = down_train.shape[1:]
    local = experts_all // n
    hidden_width = n * down_depth
    capacity = max(2, 3 * tokens // experts_all)
    chunks = model_width // hidden_width
    width = own_width // chunks
    slots = half * 2 * capacity
    dma = pltpu.SemaphoreType.DMA
    scratch = [
        pltpu.VMEM((2, local, depth, units), F32),
        pltpu.VMEM((2, tokens // PROMPT_STEPS, model_width), BF16),
        pltpu.VMEM((n - 1, local, depth, units), BF16),
        pltpu.VMEM((n - 1, local, depth, units), BF16),
        pltpu.VMEM((local, n * depth, units), BF16),
        pltpu.VMEM((local, n * depth, units), BF16),
        pltpu.VMEM((chunks, local, hidden_width, width), BF16),
        pltpu.VMEM((2, half, local, capacity, own_width), BF16),
        pltpu.VMEM((tp, local, slots, own_width), BF16),
        pltpu.VMEM((tokens, own_width), BF16),
        pltpu.VMEM((tokens, own_width), BF16),
        pltpu.VMEM((8, tokens), F32),
        pltpu.VMEM((8, tokens), F32),
        pltpu.VMEM((depth, 128), F32),
        pltpu.VMEM((tp, local, slots, units), BF16),
        pltpu.VMEM((local, slots, units), F32),
        pltpu.VMEM((2, 2, half * local * capacity, tokens), BF16),
        pltpu.VMEM((chunks, local, slots, width), BF16),
        pltpu.VMEM((chunks, 2, half, local, capacity, width), BF16),
        pltpu.VMEM((chunks, tokens, width), BF16),
        pltpu.VMEM((chunks, tokens, width), BF16),
        pltpu.VMEM((chunks, tokens, width), F32),
        pltpu.VMEM((chunks, tokens, width), BF16),
        dma((2,)),
        dma((2,)),
        dma((4,)),
        dma((11,)),
        dma((11,)),
        dma((chunks,)),
        dma((max(1, tp // 2 - 1),)),
        dma((tp // 2,)),
        dma((max(1, tp // 2 - 1),)),
        dma((tp // 2,)),
        dma((chunks,)),
        dma((chunks,)),
    ]
    any_spec = pl.BlockSpec(memory_space=pl.ANY)
    vmem_spec = pl.BlockSpec(memory_space=pltpu.VMEM)
    return pl.pallas_call(
        functools.partial(kernel, n, tp),
        out_shape=(
            jax.ShapeDtypeStruct((tokens, own_width), BF16),
            jax.ShapeDtypeStruct((local, n * depth, units), BF16),
            jax.ShapeDtypeStruct((local, n * depth, units), BF16),
            jax.ShapeDtypeStruct((local, units, model_width), BF16),
        ),
        in_specs=[any_spec] + [vmem_spec] * 4 + [any_spec] * 3,
        out_specs=(any_spec,) * 4,
        scratch_shapes=scratch,
        compiler_params=pltpu.CompilerParams(
            collective_id=0, has_side_effects=True, vmem_limit_bytes=67043328
        ),
    )(
        prompt,
        expert_ids.T,
        group_weight[None, :],
        expert_share.T,
        norm_gain[None, :],
        gate_train,
        up_train,
        down_train,
    )


def solution(mesh):
    placed = (
        P("fs", None),
        P("fs", None),
        P("fs"),
        P("fs", None),
        P("fs"),
        P(None, "fs", "tp"),
        P(None, "fs", "tp"),
        P(None, "fs", "tp"),
    )
    return jax.shard_map(
        on_device,
        mesh=mesh,
        in_specs=placed,
        out_specs=(P("fs", "tp"), P("fs", None, "tp"), P("fs", None, "tp"), P("fs", "tp", None)),
        check_vma=False,
    )
```

profile of v0, /device:TPU:0, one launch (start us, length us, event | category | flops | bytes accessed | tf_op | source)
XLA Modules:
  0.0 392.9 jit_solution(14155715867031681945)
XLA Ops:
  0.6 379.6 %shard_map.111 = (bf16[512,1024]{1,0:T(8,128)(2,1)}, bf16[2,4096,256]{2,1,0:T(8,128)(2,1)}, bf16[2,4096,256]{2,1,0:T(8,128)(2,1)}, bf16[2,256,4096]{2,1,0:T(8,128)(2,1)}) custom-call(bf16[512,4096]{1,0:T(8,128)(2,1)} %prompt.1, s32[2,512]{1,0:T(2,128)} %bitcast.4, f32[1,512]{1,0:T(1,128)} %bitcast.6, f32[2,512]{1,0:T(2,128)} %bitcast.5, f32[1,512]{1,0:T(1,128)} %bitcast.7, ...), custom_call_target="tpu_custom_call" | custom-call | tf_op jit(solution)/shard_map/pallas_call | solution.py:594
  380.3 2.3 copy.16
  382.6 0.0 copy-start.1
  382.6 4.6 %copy.17 = bf16[2,4096,256]{2,1,0:T(8,128)(2,1)} copy(bf16[2,4096,256]{2,1,0:T(8,128)(2,1)} %get-tuple-element.9) | data formatting | bytes 8388608
  387.2 0.0 copy-done.1
  387.2 0.0 copy-start
  387.2 2.1 copy.18
  389.3 1.6 copy-done
  390.9 2.0 copy.19
Async XLA Ops:
  382.6 4.6 %copy-start.1 = (bf16[2,4096,256]{2,1,0:T(8,128)(2,1)S(1)}, bf16[2,4096,256]{2,1,0:T(8,128)(2,1)}, u32[]{:S(2)}) copy-start(bf16[2,4096,256]{2,1,0:T(8,128)(2,1)} %get-tuple-element.10) | copy-start | bytes 12582916
  387.2 3.7 copy-start
where the time goes:
time: 397 us; the launch traced here: 393 us
  Pallas kernels  380 us (96%)
  local copies, waits for them, and re-layouts  12.6 us (3%)
    pallas_call x1, Pallas kernels, on_device(): pl.pallas_call(functools.partial(kernel, n, tp), out_shape=(jax.ShapeDtyp...  380 us
    unnamed x8, local copies, waits for them, and re-layouts  12.6 us

commit v1 on v0

v1 whole, which is shorter than its diff:
```python
import functools

import jax
import jax.numpy as jnp
from jax import lax
from jax.experimental import pallas as pl
from jax.experimental.pallas import tpu as pltpu
from jax.sharding import PartitionSpec as P

EPS = 1e-06
MESH = pl.DeviceIdType.MESH
BF16 = jnp.bfloat16
F32 = jnp.float32
PROMPT_STEPS = 4
AHEAD = 2


def kernel(
    n,
    tp,
    prompt,
    ids,
    group,
    share,
    gain,
    gate_hbm,
    up_hbm,
    down_hbm,
    mixed_out,
    gate_land,
    up_land,
    down_out,
    wide,
    tall,
    sends,
    down_land,
    rows_stage,
    piece,
    own_cols,
    far_cols,
    facts,
    far_facts,
    gain_cols,
    hid,
    gate_acc,
    spread,
    ret_land,
    far_stage,
    far_land,
    total,
    load_sem,
    tall_sem,
    phase_send,
    phase_recv,
    down_recv,
    send_sem,
    recv_sem,
    rows_recv,
    chip_recv,
    mate_recv,
    hid_chip_recv,
    hid_mate_recv,
    ret_recv,
    last_ret_recv,
    far_recv,
):
    here = lax.axis_index("fs")
    me = lax.axis_index("tp")
    half = n // 2
    side = here // half
    seat = here % half
    partner = (here + half) % n
    mate = me + 1 - 2 * (me % 2)
    chips = tp // 2
    tokens, model_width = prompt.shape
    experts_all, depth, units = gate_hbm.shape
    local = experts_all // n
    last = local - 1
    capacity = ret_land.shape[3]
    own_width = own_cols.shape[1]
    down_depth = down_hbm.shape[1]
    chunks, width = down_land.shape[0], down_land.shape[3]
    seat_slots = local * capacity
    slots_of_seat = 2 * capacity
    buffers, slots_sent = wide.shape[0], sends.shape[0]
    FACTS, COLS, ROWS, PIECE, HID, RET, FAR, TALL = range(8)

    def remote(src, dst, ssem, rsem, fs=None, tp_to=None):
        device = {"fs": here if fs is None else fs, "tp": me if tp_to is None else tp_to}
        return pltpu.make_async_remote_copy(
            src_ref=src,
            dst_ref=dst,
            send_sem=ssem,
            recv_sem=rsem,
            device_id=device,
            device_id_type=MESH,
        )

    def drain(ref, sem):
        pltpu.make_async_copy(ref, ref, sem).wait()

    def at(start, size, step=16):
        return pl.ds(pl.multiple_of(start, step), size)

    def shift_of(k):
        return half + (k + 1) // 2 * (1 - 2 * (k % 2))

    def owner_of(k):
        return lax.rem(here + jnp.where(k == n - 1, 0, shift_of(k)), n)

    barrier = pltpu.get_barrier_semaphore()

    @pl.loop(1, n)
    def _(s):
        pl.semaphore_signal(
            barrier, inc=1, device_id={"fs": lax.rem(here + s, n), "tp": me}, device_id_type=MESH
        )

    @pl.loop(1, tp)
    def _(s):
        pl.semaphore_signal(
            barrier, inc=1, device_id={"fs": here, "tp": lax.rem(me + s, tp)}, device_id_type=MESH
        )

    def phase_of(e, kind):
        return 3 * e + kind

    def loads(e, kind, k):
        row = owner_of(k) * local + e
        slot = k % buffers
        if kind < 2:
            source = (gate_hbm, up_hbm)[kind]
            return [pltpu.make_async_copy(source.at[row], wide.at[slot], load_sem.at[slot])]
        return [
            pltpu.make_async_copy(
                down_hbm.at[row, :, pl.ds(c * width, width)],
                wide.at[slot, pl.ds(c * down_depth, down_depth), :],
                load_sem.at[slot],
            )
            for c in range(chunks)
        ]

    def start_loads(e, kind, k):
        for copy in loads(e, kind, k):
            copy.start()

    def wait_loads(k):
        drain(wide.at[k % buffers], load_sem.at[k % buffers])

    def cast(slot, kind):
        if kind == 2:
            return [(pl.ds(0, units), wide[slot].astype(BF16))]
        return [
            (
                pl.ds(j * 128, 128),
                (wide[slot, :, pl.ds(j * 128, 128)] * gain_cols[...]).astype(BF16),
            )
            for j in range(units // 128)
        ]

    def cast_step(e, kind, k):
        wait_loads(k)
        p = phase_of(e, kind) % slots_sent
        for cols, value in cast(k % buffers, kind):
            sends[p, k, :, cols] = value

        @pl.when(k + buffers < n)
        def _():
            start_loads(e, kind, k + buffers)

    def send_matrix(e, kind, k):
        p = phase_of(e, kind)
        land = (gate_land, up_land)[kind]
        remote(
            sends.at[p % slots_sent, k],
            land.at[e, at(here * depth, depth), :],
            phase_send.at[p],
            phase_recv.at[p],
            fs=owner_of(k),
        ).start()

    def send_down(e, c):
        p = phase_of(e, 2)

        @pl.loop(0, n - 1)
        def _(k):
            remote(
                sends.at[p % slots_sent, k, at(c * down_depth, down_depth), :],
                down_land.at[c, e, at(here * down_depth, down_depth), :],
                phase_send.at[p],
                down_recv.at[c] if e == last else phase_recv.at[p],
                fs=owner_of(k),
            ).start()

    def free_slot(p):
        if p >= slots_sent:
            drain(sends.at[p % slots_sent], phase_send.at[p - slots_sent])

    def own_block(e, kind):
        k = n - 1
        wait_loads(k)
        if kind < 2:
            land = (gate_land, up_land)[kind]
            for cols, value in cast(k % buffers, kind):
                land[e, at(here * depth, depth), cols] = value
            return
        for c in range(chunks):
            down_land[c, e, at(here * down_depth, down_depth), :] = wide[
                k % buffers, pl.ds(c * down_depth, down_depth), :
            ].astype(BF16)

    def begin(e, kind):
        for k in range(min(buffers, n)):
            start_loads(e, kind, k)

    def hand_over(e, kind, first=0):
        if not first:
            free_slot(phase_of(e, kind))
            begin(e, kind)

        @pl.loop(first, n - 1)
        def _(k):
            cast_step(e, kind, k)
            if kind < 2:

                @pl.when(k > first)
                def _():
                    send_matrix(e, kind, k - 1)

        if kind < 2:
            send_matrix(e, kind, n - 2)
        else:
            for c in range(min(AHEAD, chunks) if e == last else chunks):
                send_down(e, c)
        own_block(e, kind)

    block_rows = tokens // PROMPT_STEPS

    def load_prompt(i):
        return pltpu.make_async_copy(
            prompt.at[pl.ds(i * block_rows, block_rows)], tall.at[i % 2], tall_sem.at[i % 2]
        )

    begin(0, 0)
    load_prompt(0).start()
    load_prompt(1).start()
    gain_cols[...] = jnp.transpose(jnp.broadcast_to(gain[...], (128, depth)))

    for k in range(2):
        cast_step(0, 0, k)
    pl.semaphore_wait(barrier, n - 1 + tp - 1)
    for k in range(2):
        send_matrix(0, 0, k)

    experts = lax.broadcasted_iota(jnp.int32, (experts_all, tokens), 0)
    named = [experts == ids[pl.ds(k, 1), :] for k in range(2)]
    count = sum(m.astype(F32) for m in named).astype(BF16)
    earlier = (
        lax.broadcasted_iota(jnp.int32, (tokens, tokens), 0)
        < lax.broadcasted_iota(jnp.int32, (tokens, tokens), 1)
    ).astype(F32).astype(BF16)
    ranks = jnp.dot(count, earlier, preferred_element_type=F32)
    shares = [share[pl.ds(k, 1), :] for k in range(2)]
    facts[...] = jnp.zeros_like(facts)
    for k in range(2):
        rank = jnp.sum(jnp.where(named[k], ranks, 0.0), axis=0, keepdims=True)
        facts[pl.ds(k, 1), :] = ids[pl.ds(k, 1), :].astype(F32) * capacity + rank
        facts[pl.ds(2 + k, 1), :] = group[...] * shares[k] / (shares[0] + shares[1])

    @pl.loop(0, PROMPT_STEPS)
    def _(i):
        load_prompt(i).wait()
        squares = jnp.zeros((block_rows, 128), F32)
        for j in range(model_width // 128):
            x = tall[i % 2, :, pl.ds(j * 128, 128)].astype(F32)
            squares += x * x
        mean = jnp.sum(squares, axis=1, keepdims=True) / model_width
        scale = lax.rsqrt(mean + EPS)
        own_cols[at(i * block_rows, block_rows), :] = (
            tall[i % 2, :, at(me * own_width, own_width, 128)].astype(F32) * scale
        ).astype(BF16)

        @pl.when(i + 2 < PROMPT_STEPS)
        def _():
            load_prompt(i + 2).start()

    send_facts = remote(facts, far_facts, send_sem.at[FACTS], recv_sem.at[FACTS], fs=partner)
    send_cols = remote(own_cols, far_cols, send_sem.at[COLS], recv_sem.at[COLS], fs=partner)
    send_facts.start()
    send_cols.start()

    hand_over(0, 0, 2)

    def send_rows(q, j, e):
        to = lax.rem(seat + j, half)
        remote(
            rows_stage.at[q, to, e],
            piece.at[me, e, at((seat * 2 + q) * capacity, capacity), :],
            send_sem.at[ROWS],
            rows_recv.at[e],
            fs=side * half + to,
        ).start()

    def place_rows(q, block_facts, columns):
        targets = [block_facts[pl.ds(k, 1), :].astype(jnp.int32) for k in range(2)]

        @pl.loop(0, half)
        def _(j):
            to = lax.rem(seat + j, half)
            slots = (side * half + to) * seat_slots + lax.broadcasted_iota(
                jnp.int32, (seat_slots, tokens), 0
            )
            picker = ((slots == targets[0]) | (slots == targets[1])).astype(F32).astype(BF16)
            rows = jnp.dot(picker, columns[...], preferred_element_type=F32)
            rows_stage[q, to] = rows.astype(BF16).reshape(local, capacity, own_width)

            @pl.when(j == 0)
            def _():
                piece[me, :, at((seat * 2 + q) * capacity, capacity), :] = rows_stage[q, seat]

        for e in range(local):

            @pl.loop(1, half)
            def _(j):
                send_rows(q, j, e)

    place_rows(0, facts, own_cols)
    send_facts.wait_recv()
    send_cols.wait_recv()
    place_rows(1, far_facts, far_cols)

    hand_over(0, 1)
    hand_over(0, 2)

    def spread_tp(buffer, e, which, chip_sems, mate_sems):
        mine = buffer.at[me, e]

        @pl.loop(1, chips)
        def _(j):
            remote(
                mine,
                mine,
                send_sem.at[which],
                chip_sems.at[e, j - 1],
                tp_to=lax.rem(me + 2 * j, tp),
            ).start()

        remote(mine, mine, send_sem.at[which], mate_sems.at[e, 0], tp_to=mate).start()

    def forward_tp(buffer, e, which, chip_sems, mate_sems):
        @pl.loop(1, chips)
        def _(j):
            theirs = buffer.at[lax.rem(me + tp - 2 * j, tp), e]
            drain(theirs, chip_sems.at[e, j - 1])
            remote(theirs, theirs, send_sem.at[which], mate_sems.at[e, j], tp_to=mate).start()

    def collect_tp(buffer, e, mate_sems):
        @pl.loop(0, chips)
        def _(j):
            drain(buffer.at[0, e], mate_sems.at[e, j])

    for e in range(local):
        drain(piece.at[me, e, pl.ds(0, (half - 1) * slots_of_seat), :], rows_recv.at[e])
        spread_tp(piece, e, PIECE, chip_recv, mate_recv)

    if local > 1:
        hand_over(1, 0)
        hand_over(1, 1)

    @pl.loop(0, half)
    def _(j):
        for q in range(2):
            source = (facts, far_facts)[q]
            slots = (side * half + j) * seat_slots + lax.broadcasted_iota(
                jnp.int32, (seat_slots, tokens), 0
            )
            value = sum(
                jnp.where(
                    slots == source[pl.ds(k, 1), :].astype(jnp.int32),
                    source[pl.ds(2 + k, 1), :],
                    0.0,
                )
                for k in range(2)
            )
            high = value.astype(BF16)
            spread[q, 0, at(j * seat_slots, seat_slots), :] = high
            spread[q, 1, at(j * seat_slots, seat_slots), :] = (value - high.astype(F32)).astype(
                BF16
            )

    drain(rows_stage.at[:, pl.ds(0, half - 1)], send_sem.at[ROWS])

    def contracted(land, e):
        acc = None
        for t in range(tp):
            part = jnp.dot(
                piece[t, e],
                land[e, pl.ds(t * own_width, own_width), :],
                preferred_element_type=F32,
            )
            acc = part if acc is None else acc + part
        return acc

    def hidden(e):
        forward_tp(piece, e, PIECE, chip_recv, mate_recv)
        drain(gate_land.at[e, pl.ds(0, (n - 1) * depth), :], phase_recv.at[phase_of(e, 0)])
        collect_tp(piece, e, mate_recv)
        gate_acc[...] = contracted(gate_land, e)
        drain(up_land.at[e, pl.ds(0, (n - 1) * depth), :], phase_recv.at[phase_of(e, 1)])
        up_val = contracted(up_land, e)
        g = gate_acc[...]
        hid[me, e] = (g / (1.0 + jnp.exp(-g)) * up_val).astype(BF16)
        spread_tp(hid, e, HID, hid_chip_recv, hid_mate_recv)
        forward_tp(hid, e, HID, hid_chip_recv, hid_mate_recv)
        collect_tp(hid, e, hid_mate_recv)

    def down_cols(c, e, t):
        return down_out.at[e, :, at(t * own_width + c * width, width, 128)]

    def expert_out(c, e):
        acc = None
        for t in range(tp):
            part = jnp.dot(
                hid[t, e],
                down_land[c, e, pl.ds(t * units, units), :],
                preferred_element_type=F32,
            )
            acc = part if acc is None else acc + part
        out = acc.astype(BF16).reshape(half, 2, capacity, width)
        for m in range(half):
            for q in range(2):
                rows_stage[q, m, e, :, at(c * width, width, 128)] = out[m, q]

    def turn_down(c, e):
        down_out[e, :, at(me * own_width + c * width, width, 128)] = down_land[
            c, e, at(me * units, units), :
        ]

        @pl.loop(1, tp)
        def _(j):
            to = lax.rem(me + j, tp)
            remote(
                down_land.at[c, e, at(to * units, units), :],
                down_cols(c, e, me),
                send_sem.at[TALL],
                recv_sem.at[TALL],
                tp_to=to,
            ).start()

    def send_back(e, cols, rsem):
        for q in range(2):

            @pl.loop(1, half)
            def _(j):
                to = lax.rem(seat + j, half)
                remote(
                    rows_stage.at[q, to, e, :, cols],
                    ret_land.at[q, seat, e, :, cols],
                    send_sem.at[RET],
                    rsem,
                    fs=side * half + to,
                ).start()

        for q in range(2):
            ret_land[q, seat, e, :, cols] = rows_stage[q, seat, e, :, cols]

    for e in range(last):
        hidden(e)
        p = phase_of(e, 2)
        drain(down_land.at[:, e, pl.ds(0, (n - 1) * down_depth), :], phase_recv.at[p])

        @pl.loop(0, chunks)
        def _(c):
            expert_out(c, e)

        send_back(e, pl.ds(0, own_width), ret_recv.at[e])
        hand_over(e + 1, 2)

        @pl.loop(0, chunks)
        def _(c):
            turn_down(c, e)

        if e + 2 < local:
            hand_over(e + 2, 0)
            hand_over(e + 2, 1)

    hidden(last)
    for e in range(last):
        drain(ret_land.at[:, pl.ds(0, half - 1), e], ret_recv.at[e])

    def combine(c):
        cols = at(c * width, width, 128)
        drain(ret_land.at[:, pl.ds(0, half - 1), last, :, cols], last_ret_recv.at[c])
        for q in range(2):
            back = ret_land[q, :, :, :, cols].reshape(half * seat_slots, width)
            value = sum(
                lax.dot_general(
                    spread[q, p], back, (((0,), (0,)), ((), ())), preferred_element_type=F32
                )
                for p in range(2)
            )
            if q:
                far_stage[c] = value.astype(BF16)
            else:
                total[c] = value

    def send_far(c):
        remote(
            far_stage.at[c], far_land.at[c], send_sem.at[FAR], far_recv.at[c], fs=partner
        ).start()

    @pl.loop(0, chunks)
    def _(c):
        drain(down_land.at[c, last, pl.ds(0, (n - 1) * down_depth), :], down_recv.at[c])
        expert_out(c, last)
        send_back(last, at(c * width, width, 128), last_ret_recv.at[c])

        @pl.when(c + AHEAD < chunks)
        def _():
            send_down(last, c + AHEAD)

        turn_down(c, last)

        @pl.when(c > 0)
        def _():
            combine(c - 1)
            send_far(c - 1)

    combine(chunks - 1)
    send_far(chunks - 1)

    @pl.loop(0, chunks)
    def _(c):
        drain(far_land.at[c], far_recv.at[c])
        mixed_out[:, at(c * width, width, 128)] = (
            total[c] + far_land[c].astype(F32)
        ).astype(BF16)

    for p in range(max(0, 3 * local - slots_sent), 3 * local):
        drain(sends.at[p % slots_sent], phase_send.at[p])
    send_facts.wait_send()
    send_cols.wait_send()
    drain(piece.at[pl.ds(0, 2 * chips - 1)], send_sem.at[PIECE])
    drain(hid.at[pl.ds(0, 2 * chips - 1)], send_sem.at[HID])
    drain(ret_land.at[:, pl.ds(0, half - 1)], send_sem.at[RET])
    drain(far_land, send_sem.at[FAR])
    others = down_out.at[:, :, pl.ds(0, (tp - 1) * own_width)]
    drain(others, send_sem.at[TALL])
    drain(others, recv_sem.at[TALL])


def on_device(
    prompt, expert_ids, group_weight, expert_share, norm_gain, gate_train, up_train, down_train
):
    n = lax.axis_size("fs")
    tp = lax.axis_size("tp")
    half = n // 2
    tokens, model_width = prompt.shape
    experts_all, depth, units = gate_train.shape
    down_depth, own_width = down_train.shape[1:]
    local = experts_all // n
    hidden_width = n * down_depth
    capacity = max(2, 3 * tokens // experts_all)
    chunks = model_width // hidden_width
    width = own_width // chunks
    slots = half * 2 * capacity
    dma = pltpu.SemaphoreType.DMA
    scratch = [
        pltpu.VMEM((4, depth, units), F32),
        pltpu.VMEM((2, tokens // PROMPT_STEPS, model_width), BF16),
        pltpu.VMEM((4, n - 1, depth, units), BF16),
        pltpu.VMEM((chunks, local, hidden_width, width), BF16),
        pltpu.VMEM((2, half, local, capacity, own_width), BF16),
        pltpu.VMEM((tp, local, slots, own_width), BF16),
        pltpu.VMEM((tokens, own_width), BF16),
        pltpu.VMEM((tokens, own_width), BF16),
        pltpu.VMEM((8, tokens), F32),
        pltpu.VMEM((8, tokens), F32),
        pltpu.VMEM((depth, 128), F32),
        pltpu.VMEM((tp, local, slots, units), BF16),
        pltpu.VMEM((slots, units), F32),
        pltpu.VMEM((2, 2, half * local * capacity, tokens), BF16),
        pltpu.VMEM((2, half, local, capacity, own_width), BF16),
        pltpu.VMEM((chunks, tokens, width), BF16),
        pltpu.VMEM((chunks, tokens, width), BF16),
        pltpu.VMEM((chunks, tokens, width), F32),
        dma((4,)),
        dma((2,)),
        dma((3 * local,)),
        dma((3 * local,)),
        dma((chunks,)),
        dma((8,)),
        dma((8,)),
        dma((local,)),
        dma((local, max(1, tp // 2 - 1))),
        dma((local, tp // 2)),
        dma((local, max(1, tp // 2 - 1))),
        dma((local, tp // 2)),
        dma((max(1, local - 1),)),
        dma((chunks,)),
        dma((chunks,)),
    ]
    any_spec = pl.BlockSpec(memory_space=pl.ANY)
    vmem_spec = pl.BlockSpec(memory_space=pltpu.VMEM)
    return pl.pallas_call(
        functools.partial(kernel, n, tp),
        out_shape=(
            pltpu.VMEM((tokens, own_width), BF16),
            pltpu.VMEM((local, n * depth, units), BF16),
            pltpu.VMEM((local, n * depth, units), BF16),
            pltpu.VMEM((local, units, model_width), BF16),
        ),
        in_specs=[any_spec] + [vmem_spec] * 4 + [any_spec] * 3,
        out_specs=(vmem_spec,) * 4,
        scratch_shapes=scratch,
        compiler_params=pltpu.CompilerParams(
            collective_id=0, has_side_effects=True, vmem_limit_bytes=49 << 20
        ),
    )(
        prompt,
        expert_ids.T,
        group_weight[None, :],
        expert_share.T,
        norm_gain[None, :],
        gate_train,
        up_train,
        down_train,
    )


def solution(mesh):
    placed = (
        P("fs", None),
        P("fs", None),
        P("fs"),
        P("fs", None),
        P("fs"),
        P(None, "fs", "tp"),
        P(None, "fs", "tp"),
        P(None, "fs", "tp"),
    )
    return jax.shard_map(
        on_device,
        mesh=mesh,
        in_specs=placed,
        out_specs=(P("fs", "tp"), P("fs", None, "tp"), P("fs", None, "tp"), P("fs", "tp", None)),
        check_vma=False,
    )
```

time: 397 us -> 381 us (0.960); the launches traced: 393 us -> 381 us
  Pallas kernels: 380 us -> 373 us
  local copies, waits for them, and re-layouts: 12.6 us -> 7.01 us
    pallas_call x1, Pallas kernels: 380 us -> 373 us  [on_device(): pl.pallas_call(functools.partial(kernel, n, tp), out_shape=(pltpu.VMEM((t...]
    unnamed x8 -> x4, local copies, waits for them, and re-layouts: 12.6 us -> 7.01 us
where the time goes in v1:
time: 381 us
  Pallas kernels  373 us (98%)
  local copies, waits for them, and re-layouts  7.01 us (2%)
    pallas_call x1, Pallas kernels, on_device(): pl.pallas_call(functools.partial(kernel, n, tp), out_shape=(pltpu.VMEM((t...  373 us

profile of v1, /device:TPU:0, one launch (start us, length us, event | category | flops | bytes accessed | tf_op | source)
XLA Modules:
  0.0 381.0 jit_solution(4984562209574556941)
XLA Ops:
  0.6 373.4 %shard_map.111 = (bf16[512,1024]{1,0:T(8,128)(2,1)S(1)}, bf16[2,4096,256]{2,1,0:T(8,128)(2,1)S(1)}, bf16[2,4096,256]{2,1,0:T(8,128)(2,1)S(1)}, bf16[2,256,4096]{2,1,0:T(8,128)(2,1)S(1)}) custom-call(bf16[512,4096]{1,0:T(8,128)(2,1)} %prompt.1, s32[2,512]{1,0:T(2,128)} %bitcast.4, f32[1,512]{1,0:T(1,128)} %bitcast.6, f32[2,512]{1,0:T(2,128)} %bitcast.5, ...), custom_call_target="tpu_custom_call" | custom-call | tf_op jit(solution)/shard_map/pallas_call | solution.py:605
  374.0 1.0 copy.16
  375.0 2.0 copy.17
  377.0 2.0 copy.18
  379.0 2.0 copy.19

commit v2 on v1

--- a/solution.py
+++ b/solution.py
@@ -549,6 +549,16 @@
     drain(others, recv_sem.at[TALL])
 
 
+def settle(*refs):
+    copies = [
+        pltpu.make_async_copy(refs[i], refs[4 + i], refs[8].at[i]) for i in (1, 2, 3, 0)
+    ]
+    for copy in copies:
+        copy.start()
+    for copy in copies:
+        copy.wait()
+
+
 def on_device(
     prompt, expert_ids, group_weight, expert_share, norm_gain, gate_train, up_train, down_train
 ):
@@ -602,7 +612,7 @@
     ]
     any_spec = pl.BlockSpec(memory_space=pl.ANY)
     vmem_spec = pl.BlockSpec(memory_space=pltpu.VMEM)
-    return pl.pallas_call(
+    landed = pl.pallas_call(
         functools.partial(kernel, n, tp),
         out_shape=(
             pltpu.VMEM((tokens, own_width), BF16),
@@ -626,6 +636,14 @@
         up_train,
         down_train,
     )
+    return pl.pallas_call(
+        settle,
+        out_shape=tuple(jax.ShapeDtypeStruct(x.shape, x.dtype) for x in landed),
+        in_specs=[vmem_spec] * 4,
+        out_specs=(any_spec,) * 4,
+        scratch_shapes=[dma((4,))],
+        compiler_params=pltpu.CompilerParams(vmem_limit_bytes=1 << 20),
+    )(*landed)
 
 
 def solution(mesh):

time: 381 us -> 379 us (level)
  local copies, waits for them, and re-layouts: 7.01 us -> 0 us
  Pallas kernels: 373 us -> 378 us
    unnamed x4 -> x0, local copies, waits for them, and re-layouts: 7.01 us -> none
    pallas_call x0 -> x1, Pallas kernels: none -> 4.91 us  [on_device(): pl.pallas_call(settle, out_shape=tuple((jax.ShapeDtypeStruct(x.shape, x.d...]
where the time goes in v2:
time: 379 us
  Pallas kernels  378 us (100%)
    pallas_call x1, Pallas kernels, on_device(): pl.pallas_call(functools.partial(kernel, n, tp), out_shape=(pltpu.VMEM((t...  373 us

profile of v2, /device:TPU:0, one launch (start us, length us, event | category | flops | bytes accessed | tf_op | source)
XLA Modules:
  0.0 378.9 jit_solution(9729823059238928631)
XLA Ops:
  0.6 373.4 %shard_map.111 = (bf16[512,1024]{1,0:T(8,128)(2,1)S(1)}, bf16[2,4096,256]{2,1,0:T(8,128)(2,1)S(1)}, bf16[2,4096,256]{2,1,0:T(8,128)(2,1)S(1)}, bf16[2,256,4096]{2,1,0:T(8,128)(2,1)S(1)}) custom-call(bf16[512,4096]{1,0:T(8,128)(2,1)} %prompt.1, s32[2,512]{1,0:T(2,128)} %bitcast.4, f32[1,512]{1,0:T(1,128)} %bitcast.6, f32[2,512]{1,0:T(2,128)} %bitcast.5, ...), custom_call_target="tpu_custom_call" | custom-call | tf_op jit(solution)/shard_map/pallas_call | solution.py:615
  374.0 4.9 %shard_map.112 = (bf16[512,1024]{1,0:T(8,128)(2,1)}, bf16[2,4096,256]{2,1,0:T(8,128)(2,1)}, bf16[2,4096,256]{2,1,0:T(8,128)(2,1)}, bf16[2,256,4096]{2,1,0:T(8,128)(2,1)}) custom-call(bf16[512,1024]{1,0:T(8,128)(2,1)S(1)} %get-tuple-element.8.refs_0_, bf16[2,4096,256]{2,1,0:T(8,128)(2,1)S(1)} %get-tuple-element.9.refs_1_, ...), custom_call_target="tpu_custom_call" | custom-call | tf_op jit(solution)/shard_map/pallas_call | solution.py:639

commit v3 on v2

--- a/solution.py
+++ b/solution.py
@@ -325,11 +325,11 @@
                 send_rows(q, j, e)
 
     place_rows(0, facts, own_cols)
+    hand_over(0, 1)
     send_facts.wait_recv()
     send_cols.wait_recv()
     place_rows(1, far_facts, far_cols)
 
-    hand_over(0, 1)
     hand_over(0, 2)
 
     def spread_tp(buffer, e, which, chip_sems, mate_sems):

time: 379 us -> 377 us (level)
  no operation moved by 1% of the time
where the time goes in v3:
time: 377 us
  Pallas kernels  376 us (100%)
    pallas_call x1, Pallas kernels, on_device(): pl.pallas_call(functools.partial(kernel, n, tp), out_shape=(pltpu.VMEM((t...  371 us

profile of v3, /device:TPU:0, one launch (start us, length us, event | category | flops | bytes accessed | tf_op | source)
XLA Modules:
  0.0 377.0 jit_solution(14930285166755804732)
XLA Ops:
  0.6 371.5 %shard_map.111 = (bf16[512,1024]{1,0:T(8,128)(2,1)S(1)}, bf16[2,4096,256]{2,1,0:T(8,128)(2,1)S(1)}, bf16[2,4096,256]{2,1,0:T(8,128)(2,1)S(1)}, bf16[2,256,4096]{2,1,0:T(8,128)(2,1)S(1)}) custom-call(bf16[512,4096]{1,0:T(8,128)(2,1)} %prompt.1, s32[2,512]{1,0:T(2,128)} %bitcast.4, f32[1,512]{1,0:T(1,128)} %bitcast.6, f32[2,512]{1,0:T(2,128)} %bitcast.5, ...), custom_call_target="tpu_custom_call" | custom-call | tf_op jit(solution)/shard_map/pallas_call | solution.py:615
  372.1 4.9 %shard_map.112 = (bf16[512,1024]{1,0:T(8,128)(2,1)}, bf16[2,4096,256]{2,1,0:T(8,128)(2,1)}, bf16[2,4096,256]{2,1,0:T(8,128)(2,1)}, bf16[2,256,4096]{2,1,0:T(8,128)(2,1)}) custom-call(bf16[512,1024]{1,0:T(8,128)(2,1)S(1)} %get-tuple-element.8.refs_0_, bf16[2,4096,256]{2,1,0:T(8,128)(2,1)S(1)} %get-tuple-element.9.refs_1_, ...), custom_call_target="tpu_custom_call" | custom-call | tf_op jit(solution)/shard_map/pallas_call | solution.py:639
